TPU v7x, 256 devices: a 4x2x16 block of a 4x16x16 slice. The times are simulated.
256 devices in a mesh: grp: 2 (over y), kv: 32 (over z, core), tp: 4 (over x).
Axes of the slice: x: 4, y: 2, z: 16, core: 2. Of those that a mesh axis runs over, the one named last changes fastest.
The devices are a block of a 4x16x16 slice.
Arguments:
- hidden: bfloat16 [2048, 4096], P('grp', 'kv'), parts along dimension 0, may hold values from -64 to 64
- norm_gain: bfloat16 [4096], replicated, may hold values from 0.099609375 to 1.8984375
- w_query: bfloat16 [4096, 2048], P('kv', 'tp'), may hold values from -0.09375 to 0.09375
- w_key: bfloat16 [4096, 2048], P('kv', 'tp'), may hold values from -0.09375 to 0.09375
- w_value: bfloat16 [4096, 2048], P('kv', 'tp'), may hold values from -0.09375 to 0.09375
- w_gate: bfloat16 [4096, 2048], P('kv', 'tp'), may hold values from -0.09375 to 0.09375
- w_decay: bfloat16 [4096, 16], P(None, 'tp'), may hold values from -0.09375 to 0.09375
- w_write: bfloat16 [4096, 16], P(None, 'tp'), may hold values from -0.09375 to 0.09375
- decay_rate: float32 [16], P('tp'), may hold values from 0.02 to 1
- head_gain: bfloat16 [128], replicated, may hold values from 0.099609375 to 1.8984375
- w_output: bfloat16 [2048, 4096], P('tp', 'kv'), may hold values from -0.125 to 0.125
- state: float32 [512, 16, 16384], P(('grp', 'kv'), 'tp'), parts along dimension 0, may hold values from -6 to 6
- prev_keys: bfloat16 [512, 4, 2048], P(('grp', 'kv'), None, 'tp'), parts along dimension 0, may hold values from -6 to 6
- prev_values: bfloat16 [512, 4, 2048], P(('grp', 'kv'), None, 'tp'), parts along dimension 0, may hold values from -6 to 6
- prev_decay: float32 [512, 4, 16], P(('grp', 'kv'), None, 'tp'), parts along dimension 0, may hold values from -1 to -0.02
- prev_write: float32 [512, 4, 16], P(('grp', 'kv'), None, 'tp'), parts along dimension 0, may hold values from 0.05 to 0.95
- accepted: int32 [512], P(('grp', 'kv')), parts along dimension 0, may hold values from 0 to 4
Outputs:
- mixed: bfloat16 [2048, 4096], P('grp', 'kv'), parts along dimension 0
- state_out: float32 [512, 16, 16384], P(('grp', 'kv'), 'tp'), parts along dimension 0
There are 2 independent parts, one for each index of `grp`. A program takes and returns all parts, laid end to end along the dimension named above; an argument that names none is the same for every part. Nothing has to cross between parts.
All inputs are finite; a program needn't handle non-finite values.
Results may differ from a plain program's by a relative error of at most 0.0069.
Values may be sent and summed in bfloat16 or wider, within the bound.
A program may use at most 64 MiB of HBM per device.

v0:
```python
import jax
import jax.numpy as jnp
from jax import lax
from jax.sharding import Mesh
from jax.sharding import PartitionSpec as P

KV = ("kv_0", "kv_1")
GRP_KV = ("grp", "kv_0", "kv_1")


EPSILON = 1e-06


def side_by_side(arrays, axis, dim, along):
    ends, at = ([], 0)
    for a in arrays[:-1]:
        at += a.shape[along]
        ends.append(at)
    both = jnp.concatenate(arrays, axis=along)
    return tuple(jnp.split(lax.all_gather(both, axis, axis=dim, tiled=True), ends, axis=along))


def in_order(tiles, dim):
    tiles = jnp.moveaxis(tiles, 0, dim)
    shape = tiles.shape
    return tiles.reshape(*shape[:dim], shape[dim] * shape[dim + 1], *shape[dim + 2 :])


def gather_in_order(value, axes, turns):
    tiles = value[None]
    for k in turns:
        tiles = lax.all_gather(tiles, axes[k], axis=0, tiled=True)
    block = [lax.axis_size(axes[k]) for k in reversed(turns)]
    tiles = tiles.reshape(*block, *value.shape)
    turned = sorted(range(len(turns)), key=lambda place: turns[len(turns) - 1 - place])
    return tiles.transpose(*turned, *range(len(turns), tiles.ndim)).reshape(-1, *value.shape)


def whole_of(value, axes, turns, dim):
    return in_order(gather_in_order(value, axes, turns), dim)


def from_everyone(value, axis):
    copies = jnp.broadcast_to(value, (lax.axis_size(axis), *value.shape))
    return lax.all_to_all(copies, axis, split_axis=0, concat_axis=0, tiled=True)


def of_everyone(value, axis):
    return from_everyone(value, axis).sum(axis=0)


def unit_rows(values):
    return values * lax.rsqrt(jnp.sum(values * values, axis=-1, keepdims=True) + EPSILON)


def delta_block(carried_state, keys, values, log_decay, writes, query_rows):
    length = keys.shape[2]
    totals = jnp.cumsum(log_decay, axis=-1)
    spread = totals[..., :, None] - totals[..., None, :]
    lower = jnp.tril(jnp.ones((length, length), dtype=bool))
    strict = jnp.tril(jnp.ones((length, length), dtype=bool), -1)
    within = jnp.where(lower, jnp.exp(jnp.where(lower, spread, 0.0)), 0.0)
    affinity = jnp.einsum("shid,shjd->shij", keys, keys, precision=lax.Precision.HIGHEST)
    coupling = jnp.where(strict, writes[..., :, None] * affinity * within, 0.0)
    source = jnp.concatenate(
        [values * writes[..., None], keys * (writes * jnp.exp(totals))[..., None]], axis=-1
    )
    solved = []
    for token_position in range(length):
        current = source[:, :, token_position]
        for earlier in range(token_position):
            current = current - coupling[:, :, token_position, earlier][..., None] * solved[earlier]
        solved.append(current)
    solved = jnp.stack(solved, axis=2)
    head_size = keys.shape[-1]
    fresh = solved[..., :head_size] - jnp.einsum(
        "shpk,shkv->shpv", solved[..., head_size:], carried_state, precision=lax.Precision.HIGHEST
    )
    outputs = None
    if query_rows is not None:
        scores = (
            jnp.einsum("shid,shjd->shij", query_rows, keys, precision=lax.Precision.HIGHEST)
            * within
        )
        outputs = jnp.einsum(
            "shpk,shkv->shpv",
            query_rows * jnp.exp(totals)[..., None],
            carried_state,
            precision=lax.Precision.HIGHEST,
        )
        outputs = outputs + jnp.einsum(
            "shij,shjv->shiv", scores, fresh, precision=lax.Precision.HIGHEST
        )
    final = totals[..., -1:]
    carried_state = carried_state * jnp.exp(final)[..., None] + jnp.einsum(
        "shpk,shpv->shkv",
        keys * jnp.exp(final - totals)[..., None],
        fresh,
        precision=lax.Precision.HIGHEST,
    )
    return (carried_state, outputs)


def per_device(
    hidden,
    norm_gain,
    w_query,
    w_key,
    w_value,
    w_gate,
    w_decay,
    w_write,
    decay_rate,
    head_gain,
    w_output,
    state,
    prev_keys,
    prev_values,
    prev_decay,
    prev_write,
    accepted,
):
    heads = w_decay.shape[1]
    width = w_query.shape[1]
    head_size = width // heads
    token_block = lax.all_to_all(hidden, KV, split_axis=0, concat_axis=1, tiled=True)
    wide = token_block.astype(jnp.float32)
    scaled = (wide * norm_gain.astype(jnp.float32)).astype(jnp.bfloat16)
    squares = jnp.sum(wide * wide, axis=1)
    pieces = side_by_side((w_query, w_key, w_value, w_gate), KV, 0, 1)
    summed = tuple((jnp.dot(scaled, piece, preferred_element_type=jnp.float32) for piece in pieces))
    projected = jnp.concatenate(summed, axis=1)
    small = jnp.dot(
        scaled, jnp.concatenate([w_decay, w_write], axis=1), preferred_element_type=jnp.float32
    )
    inverse = lax.rsqrt(squares / norm_gain.shape[0] + EPSILON)
    projected = projected * inverse[:, None]
    small = small * inverse[:, None]
    seqs = state.shape[0]
    proposals = projected.shape[0] // seqs

    def heads_first(block):
        return block.reshape(seqs, proposals, heads, head_size).transpose(0, 2, 1, 3)

    query_rows = unit_rows(heads_first(projected[:, :width])) * head_size ** (-0.5)
    keys = unit_rows(heads_first(projected[:, width : 2 * width]))
    values = heads_first(projected[:, 2 * width : 3 * width])
    gates = projected[:, 3 * width :].reshape(seqs, proposals, heads, head_size)
    log_decay = (
        (-decay_rate * jax.nn.softplus(small[:, :heads]))
        .reshape(seqs, proposals, heads)
        .transpose(0, 2, 1)
    )
    writes = jax.nn.sigmoid(small[:, heads:]).reshape(seqs, proposals, heads).transpose(0, 2, 1)
    taken = jnp.arange(proposals, dtype=jnp.int32)[None, :] < accepted[:, None]
    old_keys = unit_rows(
        prev_keys.astype(jnp.float32)
        .reshape(seqs, proposals, heads, head_size)
        .transpose(0, 2, 1, 3)
    )
    old_values = (
        prev_values.astype(jnp.float32)
        .reshape(seqs, proposals, heads, head_size)
        .transpose(0, 2, 1, 3)
    )
    old_decay = jnp.where(taken[:, :, None], prev_decay, 0.0).transpose(0, 2, 1)
    old_writes = jnp.where(taken[:, :, None], prev_write, 0.0).transpose(0, 2, 1)
    carried_state = state.reshape(seqs, heads, head_size, head_size)
    carried_state, _ = delta_block(carried_state, old_keys, old_values, old_decay, old_writes, None)
    _, outputs = delta_block(carried_state, keys, values, log_decay, writes, query_rows)
    outputs = outputs.transpose(0, 2, 1, 3)
    normed = outputs * lax.rsqrt(jnp.mean(outputs * outputs, axis=-1, keepdims=True) + EPSILON)
    normed = normed * head_gain.astype(jnp.float32) * jax.nn.silu(gates)
    heads_out = normed.reshape(seqs * proposals, width).astype(jnp.bfloat16)
    terms = jnp.dot(
        whole_of(heads_out, KV, (0, 1), 0), w_output, preferred_element_type=jnp.float32
    )
    mixed = of_everyone(terms, "tp").astype(jnp.bfloat16)
    return (mixed, carried_state.reshape(seqs, heads, head_size * head_size))


def solution(mesh):
    torus = Mesh(
        mesh.devices.reshape(mesh.shape["grp"], 16, 2, mesh.shape["tp"]),
        ("grp", "kv_0", "kv_1", "tp"),
    )
    in_specs = (
        P("grp", KV),
        P(),
        P(KV, "tp"),
        P(KV, "tp"),
        P(KV, "tp"),
        P(KV, "tp"),
        P(None, "tp"),
        P(None, "tp"),
        P("tp"),
        P(),
        P("tp", KV),
        P(GRP_KV, "tp", None),
        P(GRP_KV, None, "tp"),
        P(GRP_KV, None, "tp"),
        P(GRP_KV, None, "tp"),
        P(GRP_KV, None, "tp"),
        P(GRP_KV),
    )
    out_specs = (P("grp", KV), P(GRP_KV, "tp", None))
    return jax.shard_map(
        per_device, mesh=torus, in_specs=in_specs, out_specs=out_specs, check_vma=False
    )
```

profile of v0, /device:TPU:40, one launch (start us, length us, event | category | flops | bytes accessed | tf_op | source)
XLA Modules:
  0.0 249.6 jit_solution(17397073867392320041)
XLA Ops:
  7.3 2.0 pad_maximum_fusion
  9.4 24.8 %all-to-all-start = ((bf16[32,32,128]{2,1,0:T(8,128)(2,1)}), bf16[32,32,128]{2,1,0:T(8,128)(2,1)S(1)}, u32[]{:S(2)}, u32[]{:S(2)}) async-start(bf16[32,32,128]{2,1,0:T(8,128)(2,1)} %bitcast.155), calls=%async_computation | async-start | bytes 524288 | tf_op jit(solution)/shard_map/all_to_all | solution.py:126
  34.4 0.1 copy.357
  34.5 0.1 copy.354
  34.6 0.1 copy.355
  34.7 0.1 fusion.31
  34.9 0.4 fusion.11
  35.4 0.2 fusion.19
  35.6 0.2 fusion.79
  35.8 2.7 %reshape.141 = f32[8,4,128,128]{3,2,1,0:T(8,128)S(1)} reshape(f32[8,4,16384]{2,1,0:T(4,128)} %param.28) | data formatting | bytes 4194304 | tf_op jit(solution)/shard_map/reshape | solution.py:168
  38.5 0.1 copy.369
  39.7 0.1 copy.353
  39.8 0.3 multiply_subtract_fusion.2
  40.1 0.1 pad_maximum_fusion.1
  40.2 1.9 convolution_subtract_fusion.1
  42.1 5.3 %multiply_add_fusion = f32[8,4,128,128]{3,2,1,0:T(8,128)S(1)} fusion(f32[8,4,128,128]{3,2,1,0:T(8,128)} %copy-done.1, f32[8,4,4,128]{3,2,1,0:T(4,128)S(1)} %convolution_subtract_fusion.1, f32[8,4]{1,0:T(8,128)S(1)} %copy.352, bf16[8,4,512]{2,1,0:T(4,128)(2,1)S(1)} %copy-done.2, f32[8,4,4]{2,1,0:T(4,128)S(1)} %copy.353, f32[8,4,4]{2,1,0:T(4,128)S(1)} %add_rsqrt_fusion.2), kind=kOutput, calls=%fused_computation.8 | convolution fusion | flops 26263552 | bytes 4293760 | tf_op jit(solution)/shard_map/shpk,shpv->shkv/dot_general | solution.py:95
  47.4 10.6 %all-to-all-done = bf16[32,32,128]{2,1,0:T(8,128)(2,1)S(1)} async-done(((bf16[32,32,128]{2,1,0:T(8,128)(2,1)}), bf16[32,32,128]{2,1,0:T(8,128)(2,1)S(1)}, u32[]{:S(2)}, u32[]{:S(2)}) %all-to-all-start) | async-done | bytes 262176 | tf_op jit(solution)/shard_map/all_to_all | solution.py:126
  58.0 0.2 fusion.12
  58.2 0.2 convolution_multiply_fusion.3
  58.6 0.7 reduce_window_sum.17
  59.4 75.7 %all-gather.3.cloned.1.call-done = bf16[4096,2048]{1,0:T(8,128)(2,1)} async-done(((bf16[128,2048]{1,0:T(8,128)(2,1)}), bf16[4096,2048]{1,0:T(8,128)(2,1)}) %all-gather.3.cloned.1.call-update) | async-done | bytes 16777232 | tf_op jit(solution)/shard_map/all_gather | solution.py:20
  135.0 3.0 %fusion = f32[32,512]{1,0:T(8,128)S(1)} fusion(bf16[4096,2048]{1,0:T(8,128)(2,1)} %all-gather.3.cloned.1.call-done, f32[4096]{0:T(1024)S(1)} %convert_element_type.43, bf16[32,32,128]{2,1,0:T(8,128)(2,1)S(1)} %all-to-all-done), kind=kOutput, calls=%fused_computation | convolution fusion | flops 134610944 | bytes 4538368 | tf_op jit(solution)/shard_map/dot_general | solution.py:131
  138.0 3.0 %fusion.2 = f32[32,512]{1,0:T(8,128)S(1)} fusion(bf16[4096,2048]{1,0:T(8,128)(2,1)} %all-gather.3.cloned.1.call-done, f32[4096]{0:T(1024)S(1)} %convert_element_type.43, bf16[32,32,128]{2,1,0:T(8,128)(2,1)S(1)} %all-to-all-done), kind=kOutput, calls=%fused_computation.2 | convolution fusion | flops 134610944 | bytes 4538368 | tf_op jit(solution)/shard_map/dot_general | solution.py:131
  141.0 3.0 %fusion.4 = f32[32,512]{1,0:T(8,128)S(1)} fusion(bf16[4096,2048]{1,0:T(8,128)(2,1)} %all-gather.3.cloned.1.call-done, f32[4096]{0:T(1024)S(1)} %convert_element_type.43, bf16[32,32,128]{2,1,0:T(8,128)(2,1)S(1)} %all-to-all-done), kind=kOutput, calls=%fused_computation.4 | convolution fusion | flops 134610944 | bytes 4538368 | tf_op jit(solution)/shard_map/dot_general | solution.py:131
  144.0 3.0 %fusion.6 = f32[32,512]{1,0:T(8,128)S(1)} fusion(bf16[4096,2048]{1,0:T(8,128)(2,1)} %all-gather.3.cloned.1.call-done, f32[4096]{0:T(1024)S(1)} %convert_element_type.43, bf16[32,32,128]{2,1,0:T(8,128)(2,1)S(1)} %all-to-all-done), kind=kOutput, calls=%fused_computation.6 | convolution fusion | flops 134610944 | bytes 4538368 | tf_op jit(solution)/shard_map/dot_general | solution.py:131
  147.3 0.1 fusion.24
  147.4 0.1 fusion.32
  147.6 0.1 fusion.38
  147.7 0.4 convolution_multiply_fusion.1
  148.2 0.4 fusion.9
  148.7 0.2 fusion.78
  150.0 0.3 multiply_subtract_fusion
  150.3 0.1 pad_maximum_fusion.2
  150.4 1.9 convolution_subtract_fusion
  152.3 1.9 fusion.34
  154.2 0.4 fusion.80
  154.5 0.1 fusion.20
  154.7 0.1 copy.393
  154.8 0.1 copy.394
  155.0 33.1 %all_gather.10 = bf16[16,32,512]{2,1,0:T(8,128)(2,1)} all-gather(bf16[1,32,512]{2,1,0:T(8,128)(2,1)S(1)} %convert_element_type.48), channel_id=1, replica_groups=mesh['grp'=2,'kv_0'=16,'kv_1'=2,'tp'=4] {'kv_0'}, dimensions={0}, use_global_device_ids=true | all-gather | bytes 557056 | tf_op jit(solution)/shard_map/all_gather | solution.py:32
  188.2 17.3 %all-gather.5.cloned.1.call-done = bf16[32,32,512]{2,1,0:T(8,128)(2,1)} async-done(((bf16[16,32,512]{2,1,0:T(8,128)(2,1)}), bf16[32,32,512]{2,1,0:T(8,128)(2,1)}) %all-gather.5.cloned.1.call-update) | async-done | bytes 1048592 | tf_op jit(solution)/shard_map/all_gather | solution.py:32
  205.4 1.3 copy.398
  206.8 0.4 fusion.81
  207.2 1.5 broadcast_in_dim.79
  208.7 4.5 %all-to-all-start.1 = ((f32[4,1024,128]{2,1,0:T(8,128)}), f32[4,1024,128]{2,1,0:T(8,128)}, u32[]{:S(2)}, u32[]{:S(2)}) async-start(f32[4,1024,128]{2,1,0:T(8,128)} %broadcast_in_dim.79), calls=%async_computation.1 | async-start | bytes 4194304 | tf_op jit(solution)/shard_map/all_to_all | solution.py:45
  213.2 1.9 reshape.149
  215.1 25.2 %all-to-all-done.1 = f32[4,1024,128]{2,1,0:T(8,128)} async-done(((f32[4,1024,128]{2,1,0:T(8,128)}), f32[4,1024,128]{2,1,0:T(8,128)}, u32[]{:S(2)}, u32[]{:S(2)}) %all-to-all-start.1) | async-done | bytes 2097184 | tf_op jit(solution)/shard_map/all_to_all | solution.py:45
  240.3 2.5 reduce_sum.59
  (83 shorter events, 3.4 us)
Async XLA Ops:
  7.2 199.6 %copy-start = (bf16[512,128]{1,0:T(8,128)(2,1)S(1)}, bf16[512,128]{1,0:T(8,128)(2,1)}, u32[]{:S(2)}) copy-start(bf16[512,128]{1,0:T(8,128)(2,1)} %param.27) | copy-start | bytes 393220
  7.2 27.1 %copy-start.9 = (s32[8]{0:T(128)S(1)}, s32[8]{0:T(128)}, u32[]{:S(2)}) copy-start(s32[8]{0:T(128)} %param.33) | copy-start | bytes 100
  7.2 27.1 %copy-start.5 = (f32[8,4,4]{0,2,1:T(4,128)S(1)}, f32[8,4,4]{0,2,1:T(4,128)}, u32[]{:S(2)}) copy-start(f32[8,4,4]{0,2,1:T(4,128)} %param.31) | copy-start | bytes 1540
  7.2 27.2 %copy-start.6 = (f32[8,4,4]{0,2,1:T(4,128)S(1)}, f32[8,4,4]{0,2,1:T(4,128)}, u32[]{:S(2)}) copy-start(f32[8,4,4]{0,2,1:T(4,128)} %param.32) | copy-start | bytes 1540
  7.2 27.5 %copy-start.2 = (bf16[8,4,512]{2,1,0:T(4,128)(2,1)S(1)}, bf16[8,4,512]{2,1,0:T(4,128)(2,1)}, u32[]{:S(2)}) copy-start(bf16[8,4,512]{2,1,0:T(4,128)(2,1)} %param.29) | copy-start | bytes 98308
  7.2 28.1 %copy-start.3 = (bf16[8,4,512]{2,1,0:T(4,128)(2,1)S(1)}, bf16[8,4,512]{2,1,0:T(4,128)(2,1)}, u32[]{:S(2)}) copy-start(bf16[8,4,512]{2,1,0:T(4,128)(2,1)} %param.30) | copy-start | bytes 98308
  7.2 28.5 %copy-start.4 = (bf16[4096]{0:T(1024)(128)(2,1)S(1)}, bf16[4096]{0:T(1024)(128)(2,1)}, u32[]{:S(2)}) copy-start(bf16[4096]{0:T(1024)(128)(2,1)} %param.18) | copy-start | bytes 24580
  7.3 28.5 %copy-start.10 = (bf16[128]{0:T(256)(128)(2,1)S(1)}, bf16[128]{0:T(256)(128)(2,1)}, u32[]{:S(2)}) copy-start(bf16[128]{0:T(256)(128)(2,1)} %param.26) | copy-start | bytes 772
  7.3 28.5 %copy-start.11 = (f32[4]{0:T(128)S(1)}, f32[4]{0:T(128)}, u32[]{:S(2)}) copy-start(f32[4]{0:T(128)} %param.25) | copy-start | bytes 52
  7.3 127.8 %all-gather.3.cloned.1.call-start = ((), (), s32[]{:S(2)}) async-start(), calls=%async_computation.2 | async-start | bytes 17301504 | tf_op jit(solution)/shard_map/all_gather | solution.py:20
  9.4 48.7 %all-to-all-start = ((bf16[32,32,128]{2,1,0:T(8,128)(2,1)}), bf16[32,32,128]{2,1,0:T(8,128)(2,1)S(1)}, u32[]{:S(2)}, u32[]{:S(2)}) async-start(bf16[32,32,128]{2,1,0:T(8,128)(2,1)} %bitcast.155), calls=%async_computation | async-start | bytes 524288 | tf_op jit(solution)/shard_map/all_to_all | solution.py:126
  34.2 171.2 %all-gather.5.cloned.1.call-start = ((), (), s32[]{:S(2)}) async-start(), calls=%async_computation.3 | async-start | bytes 1572864 | tf_op jit(solution)/shard_map/all_gather | solution.py:32
  38.5 1.8 copy-start.1
  42.1 16.1 %copy-start.7 = (bf16[4096,4]{0,1:T(4,128)(2,1)S(1)}, bf16[4096,4]{0,1:T(4,128)(2,1)}, u32[]{:S(2)}) copy-start(bf16[4096,4]{0,1:T(4,128)(2,1)} %param.24) | copy-start | bytes 98308
  42.1 16.1 %copy-start.8 = (bf16[4096,4]{0,1:T(4,128)(2,1)S(1)}, bf16[4096,4]{0,1:T(4,128)(2,1)}, u32[]{:S(2)}) copy-start(bf16[4096,4]{0,1:T(4,128)(2,1)} %param.23) | copy-start | bytes 98308
  208.7 31.6 %all-to-all-start.1 = ((f32[4,1024,128]{2,1,0:T(8,128)}), f32[4,1024,128]{2,1,0:T(8,128)}, u32[]{:S(2)}, u32[]{:S(2)}) async-start(f32[4,1024,128]{2,1,0:T(8,128)} %broadcast_in_dim.79), calls=%async_computation.1 | async-start | bytes 4194304 | tf_op jit(solution)/shard_map/all_to_all | solution.py:45
Sparse Core Ops, SparseCore 0:
  10.0 125.0 all-gather.2
  188.3 17.0 all-gather.4
where the time goes:
time: 252 us; the launch traced here: 250 us
  waiting for transfers between devices  129 us (51%)
  blocking collectives  33.1 us (13%)
  starting transfers between devices  29.5 us (12%)
  matrix products  25.2 us (10%)
  between operations  14.6 us (6%)
  local copies, waits for them, and re-layouts  11 us (4%)
  other arithmetic  7.45 us (3%)
    all_gather x1, waiting for transfers between devices, side_by_side(): lax.all_gather(both, axis, axis=dim, tiled=True)  75.7 us
    all_gather x1, blocking collectives, gather_in_order(): tiles = lax.all_gather(tiles, axes[k], axis=0, tiled=True)  33.1 us
    all_to_all x1, waiting for transfers between devices, from_everyone(): return lax.all_to_all(copies, axis, split_axis=0, concat_axis=0, tiled=True)  25.2 us
    all_to_all x1, starting transfers between devices, per_device(): lax.all_to_all(hidden, KV, split_axis=0, concat_axis=1, tiled=True)  24.8 us
    all_gather x1, waiting for transfers between devices, gather_in_order(): tiles = lax.all_gather(tiles, axes[k], axis=0, tiled=True)  17.3 us
    dot_general x4, matrix products, per_device(): jnp.dot(scaled, piece, preferred_element_type=jnp.float32)  12 us
    all_to_all x1, waiting for transfers between devices, per_device(): lax.all_to_all(hidden, KV, split_axis=0, concat_axis=1, tiled=True)  10.6 us
    dot_general x1, matrix products, delta_block(): jnp.einsum('shpk,shpv->shkv', keys * jnp.exp(final - totals)[..., None],...  5.32 us
  transfers between devices with their start and end apart: 4, of which 4 were waited for; matrix products, arithmetic and copies ran while one was open for 6% of the time, Pallas kernels for 0%

commit v1 on v0

v1 whole, which is shorter than its diff:
```python
import functools

import jax
import jax.numpy as jnp
from jax import lax
from jax.experimental import pallas as pl
from jax.experimental.pallas import tpu as pltpu
from jax.sharding import PartitionSpec as P

MESH = pl.DeviceIdType.MESH
GRP_KV = ("grp", "kv")
EPSILON = 1e-06
F32 = jnp.float32
BF16 = jnp.bfloat16
PIECES = 4
WIDE_HOPS = 1
RELAY = 2


def split(value):
    high = value.astype(BF16)
    return high, (value - high.astype(F32)).astype(BF16)


def dot(a, b, dims=((1,), (0,))):
    return lax.dot_general(a, b, (dims, ((), ())), preferred_element_type=F32)


def lane_sum(value):
    return jnp.sum(value, axis=-1, keepdims=True)


def body(
    sizes,
    hidden, gain, w_query, w_key, w_value, w_gate, w_decay, w_write, rate, head_gain, w_output,
    state, prev_keys, prev_values, old_scalars,
    mixed, state_out,
    raw, gains, scaled, held_w, sent_w, squares, weights_small, partial,
    out_bf, in_bf, out_wide, in_wide, out_small, in_small,
    sums, halves, small, small_t,
    s_old, s_high, s_low, s_new, old_k, old_v, reads, rows_k, rows_u,
    heads_f32, heads_bf, gathered, flat, w_out_all, result,
    load_sem, pair_send, pair_recv, ring_send, ring_recv, swap_send, swap_recv,
    w_send, w_recv, head_send, head_recv, relay_send, relay_recv, twin_send, twin_recv,
    mix_send, mix_recv, store_sem,
):
    zs, tps, seqs, props, heads, hs = sizes
    half = zs // 2
    kv = lax.axis_index("kv")
    tp = lax.axis_index("tp")
    z = kv // 2
    core = lax.rem(kv, 2)
    other = 1 - core
    twin = z * 2 + other
    width = heads * hs
    rows = scaled.shape[0] // zs
    mine = rows // 2
    feats = hidden.shape[1]
    part = held_w.shape[1] // PIECES
    model = gain.shape[0] * gain.shape[1]

    def at_z(step):
        return lax.rem(z + step + 2 * zs, zs)

    def kv_at(step):
        return at_z(step) * 2 + core

    def tp_at(step):
        return lax.rem(tp + step, tps)

    def remote(src, dst, send, recv, **where):
        return pltpu.make_async_remote_copy(
            src_ref=src, dst_ref=dst, send_sem=send, recv_sem=recv, device_id=where, device_id_type=MESH
        )

    loads = [
        pltpu.make_async_copy(hidden, raw.at[0], load_sem.at[0]),
        pltpu.make_async_copy(w_output, w_out_all.at[tp], load_sem.at[1]),
        pltpu.make_async_copy(state, s_old, load_sem.at[2]),
    ]
    for load in loads:
        load.start()

    def weight_loads(first, second):
        return [
            pltpu.make_async_copy(first[0], held_w.at[pl.ds(0, feats), pl.ds(0, width)], load_sem.at[3]),
            pltpu.make_async_copy(first[1], held_w.at[pl.ds(0, feats), pl.ds(width, width)], load_sem.at[4]),
            pltpu.make_async_copy(second[0], sent_w.at[:, pl.ds(0, width)], load_sem.at[5]),
            pltpu.make_async_copy(second[1], sent_w.at[:, pl.ds(width, width)], load_sem.at[6]),
        ]

    by_core = (
        weight_loads((w_query, w_key), (w_gate, w_value)),
        weight_loads((w_gate, w_value), (w_query, w_key)),
    )
    for k in range(2):
        @pl.when(core == k)
        def _():
            for load in by_core[k]:
                load.start()

    barrier = pltpu.get_barrier_semaphore()
    near = [twin] + [kv_at(d * h) for h in range(1, RELAY + 1) for d in (1, -1)]
    for peer in near:
        pl.semaphore_signal(barrier, inc=1, device_id={"kv": peer}, device_id_type=MESH)
    for step in range(1, tps):
        pl.semaphore_signal(barrier, inc=1, device_id={"tp": tp_at(step)}, device_id_type=MESH)

    gains[...] = gain[...].astype(F32)
    small[...] = jnp.zeros_like(small)
    at_own = pl.multiple_of(kv * feats, feats)
    at_twin = pl.multiple_of(twin * feats, feats)
    for k, small_weight in enumerate((w_decay, w_write)):
        @pl.when(core == k)
        def _():
            w = jnp.concatenate(
                [small_weight[:, pl.ds(at_own, feats)], small_weight[:, pl.ds(at_twin, feats)]], axis=1
            )
            weights_small[0:heads, :] = w.astype(F32)
    weights_small[heads:, :] = jnp.zeros((8 - heads, 2 * feats), F32)

    pl.semaphore_wait(barrier, len(near) + tps - 1)

    loads[0].wait()
    for load in by_core[0]:
        load.wait()
    pair = [
        remote(raw.at[0], raw.at[1], pair_send.at[0], pair_recv.at[0], kv=twin),
        remote(sent_w, held_w.at[pl.ds(feats, feats), :], pair_send.at[1], pair_recv.at[1], kv=twin),
    ]
    for copy in pair:
        copy.start()
    loads[1].wait()
    w_copies = []
    for step in range(1, tps):
        w_copies.append(
            remote(w_out_all.at[tp], w_out_all.at[tp], w_send.at[step - 1], w_recv.at[step - 1], tp=tp_at(step))
        )
        w_copies[-1].start()

    def scale(slot, who):
        wide = raw[slot].astype(F32)
        scaled[:, slot * feats:(slot + 1) * feats] = (wide * gains[pl.ds(who, 1), :]).astype(BF16)
        wide = wide * wide
        squares[0, :, slot * feats:(slot + 1) * feats], squares[1, :, slot * feats:(slot + 1) * feats] = split(wide)

    scale(0, kv)
    for copy in pair:
        copy.wait()
    scale(1, twin)

    w_small = weights_small[...].astype(BF16)
    ones_row = (lax.broadcasted_iota(jnp.int32, (8, 2 * feats), 0) == heads).astype(BF16)

    def chunk_dot(chunk, slot):
        at = pl.ds(pl.multiple_of(chunk * rows, rows), rows)
        partial[slot] = dot(scaled[at, :], held_w[...])

    def small_dot(chunk):
        at = pl.ds(pl.multiple_of(chunk * rows, rows), rows)
        over = ((1,), (1,))
        return (
            dot(w_small, scaled[at, :], over)
            + dot(ones_row, squares[0, at, :], over)
            + dot(ones_row, squares[1, at, :], over)
        )

    taken_reads = []
    old = {}

    def old_reads(seq):
        for h in range(heads):
            matrix = s_old[pl.ds(seq * hs * heads + h, hs, stride=heads), :]
            high, low = split(matrix)
            key_rows = old_k[h, seq * props:(seq + 1) * props, :]
            key_rows = jnp.concatenate([key_rows, jnp.zeros_like(key_rows)], axis=0).astype(BF16)
            reads[h, seq * 8:(seq + 1) * 8, :] = dot(key_rows, high) + dot(key_rows, low)

    def by_head(fn):
        return jnp.concatenate([fn(h) for h in range(heads)], axis=1)

    def load_rows(ref, at):
        return by_head(lambda h: ref[h, at, :])

    def store_rows(ref, at, value):
        for h in range(heads):
            ref[h, at, :] = head(value, h)

    def head(value, h):
        return value[:, h * hs:(h + 1) * hs]

    def spread(value):
        return by_head(lambda h: jnp.broadcast_to(value[:, h:h + 1], (seqs, hs)))

    def head_sums(value):
        return by_head(lambda h: jnp.broadcast_to(lane_sum(head(value, h)), (seqs, hs)))

    def unit(value):
        return value * lax.rsqrt(head_sums(value) + EPSILON)

    def unit_factor(value):
        return lax.rsqrt(head_sums(value) + EPSILON)

    def updates(keys, values, log_decay, writes, state_reads):
        totals, fresh = [], []
        for p in range(props):
            totals.append(log_decay[p] if p == 0 else totals[-1] + log_decay[p])
            value = values[p] - jnp.exp(totals[p]) * state_reads[p]
            for e in range(p):
                value = value - jnp.exp(totals[p] - totals[e]) * head_sums(keys[p] * keys[e]) * fresh[e]
            fresh.append(writes[p] * value)
        return totals, fresh

    def old_updates():
        keys, values, log_decay, writes, state_reads = [], [], [], [], []
        for p in range(props):
            key = load_rows(old_k, pl.ds(p, seqs, stride=props))
            factor = unit_factor(key * key)
            keys.append(key * factor)
            values.append(load_rows(old_v, pl.ds(p, seqs, stride=props)))
            log_decay.append(spread(old_scalars[:, p * heads:(p + 1) * heads]))
            writes.append(spread(old_scalars[:, (props + p) * heads:(props + p + 1) * heads]))
            state_reads.append(load_rows(reads, pl.ds(p, seqs, stride=8)) * factor)
        totals, fresh = updates(keys, values, log_decay, writes, state_reads)
        for p in range(props):
            store_rows(rows_k, pl.ds(p, seqs, stride=props), jnp.exp(totals[-1] - totals[p]) * keys[p])
            store_rows(rows_u, pl.ds(p, seqs, stride=props), fresh[p])
        old["decay"] = jnp.exp(totals[-1])

    def old_state(seq):
        for h in range(heads):
            at = pl.ds(seq * hs * heads + h, hs, stride=heads)
            k4 = rows_k[h, seq * props:(seq + 1) * props, :]
            u4 = rows_u[h, seq * props:(seq + 1) * props, :]
            k_high, u_high = k4.astype(BF16).astype(F32), u4.astype(BF16).astype(F32)
            lhs = jnp.concatenate([k_high, k4 - k_high, k_high, jnp.zeros_like(k4)], axis=0).astype(BF16)
            rhs = jnp.concatenate([u_high, u_high, u4 - u_high, jnp.zeros_like(u4)], axis=0).astype(BF16)
            matrix = s_old[at, :] * rows_u[h, seqs * props + seq:seqs * props + seq + 1, :] + dot(lhs, rhs, ((0,), (0,)))
            s_new[at, :] = matrix
            s_high[seq * heads + h], s_low[seq * heads + h] = split(matrix)

    stores = [
        pltpu.make_async_copy(
            s_new.at[pl.ds(s * hs * heads, hs * heads), :],
            state_out.at[pl.ds(s * hs * heads, hs * heads), :],
            store_sem.at[s],
        )
        for s in range(seqs)
    ]

    def side_work(step):
        if step == 1:
            loads[2].wait()
            for s in range(seqs):
                store_rows(old_k, pl.ds(s * props, props), prev_keys[s].astype(F32))
                store_rows(old_v, pl.ds(s * props, props), prev_values[s].astype(F32))
        if step in (1, 2):
            for s in range((step - 1) * seqs // 2, step * seqs // 2):
                old_reads(s)
        if step == 3:
            old_updates()
            store_rows(rows_u, pl.ds(seqs * props, seqs), old["decay"])
        if 4 <= step:
            per = seqs // (half - 4)
            for s in range((step - 4) * per, (step - 3) * per):
                old_state(s)
                stores[s].start()

    def is_wide(step, piece):
        return piece < PIECES // 2 and step >= half - WIDE_HOPS

    ring = {}

    def place(step, side, piece):
        if piece == PIECES:
            return out_small.at[step, side], in_small.at[step, side]
        if is_wide(step, piece):
            return (
                out_wide.at[step - half + WIDE_HOPS, side, piece],
                in_wide.at[step - half + WIDE_HOPS, side, piece],
            )
        return out_bf.at[step, side, piece], in_bf.at[step, side, piece]

    def first_step(side, piece):
        return 0 if piece % 2 == side else 1

    for step in range(half):
        chunk_dot(at_z(half - step), 0)
        if step > 0:
            chunk_dot(at_z(step - half), 1)
        small_part = [small_dot(at_z(half - step)), small_dot(at_z(step - half)) if step > 0 else None]
        side_work(step)
        for piece in range(PIECES + 1):
            for side in range(2):
                begins = first_step(side, piece)
                if step < begins:
                    continue
                if piece == PIECES:
                    value = small_part[side]
                else:
                    value = partial[side if step > 0 else 0, :, piece * part:(piece + 1) * part]
                if step > begins:
                    before = ring[step - 1, side, piece]
                    before.wait_recv()
                    value = value + place(step - 1, side, piece)[1][...].astype(F32)
                src, dst = place(step, side, piece)
                src[...] = value.astype(src.dtype)
                copy = remote(
                    src, dst,
                    ring_send.at[step, side, piece], ring_recv.at[step, side, piece],
                    kv=kv_at(1 - 2 * side),
                )
                copy.start()
                ring[step, side, piece] = copy
    chunk_dot(z, 0)
    own_small = small_dot(z)
    swaps = []
    for piece in range(PIECES + 1):
        value = own_small if piece == PIECES else partial[0, :, piece * part:(piece + 1) * part]
        for side in range(2):
            ring[half - 1, side, piece].wait_recv()
            value = value + place(half - 1, side, piece)[1][...].astype(F32)
        if piece == PIECES:
            small[core, :, 0:rows] = value
        else:
            blocks = pl.ds(piece * (part // hs), part // hs)
            for n in range(part // hs):
                for owner in range(2):
                    sums[owner, piece * (part // hs) + n] = value[owner * mine:(owner + 1) * mine, n * hs:(n + 1) * hs]
            swap = remote(
                sums.at[other, blocks], halves.at[core, blocks], swap_send.at[piece], swap_recv.at[piece], kv=twin
            )
            swap.start()
            swaps.append(swap)
    swap = remote(small.at[core], small.at[core], swap_send.at[PIECES], swap_recv.at[PIECES], kv=twin)
    swap.start()
    swaps.append(swap)
    halves[core] = sums[core]
    for swap in swaps:
        swap.wait()

    for k in range(2):
        small_t[k, :, 0:8] = jnp.transpose(small[k])

    def piece_of(kind, at):
        return by_head(lambda h: halves[kind // 2, (kind % 2) * heads + h, at, :])

    for s in range(seqs):
        at = pl.ds(s * props, props)
        q4, k4 = piece_of(0, at), piece_of(1, at)
        for h in range(heads):
            cols = slice(h * hs, (h + 1) * hs)
            lhs = jnp.concatenate([q4[:, cols], k4[:, cols]], axis=0)
            high = lhs.astype(BF16).astype(F32)
            both = jnp.concatenate([high, lhs - high], axis=0).astype(BF16)
            first = dot(both, s_high[s * heads + h])
            second = dot(high.astype(BF16), s_low[s * heads + h])
            reads[h, s * 8:(s + 1) * 8, :] = first[:8] + first[8:] + second

    queries, keys, values, log_decay, writes, reads_q, reads_k, gates = ([] for _ in range(8))
    rates = jnp.broadcast_to(rate[...], (seqs, heads))
    for p in range(props):
        at = pl.ds(p, seqs, stride=props)
        at_small = pl.ds(core * mine + p, seqs, stride=props)
        cols_d, cols_w = small_t[0, at_small, :], small_t[1, at_small, :]
        inverse = lax.rsqrt(cols_d[:, heads:heads + 1] * (1.0 / model) + EPSILON)
        pre_decay = cols_d[:, 0:heads] * inverse
        pre_write = cols_w[:, 0:heads] * inverse
        soft = jnp.maximum(pre_decay, 0.0) + jnp.log1p(jnp.exp(-jnp.abs(pre_decay)))
        log_decay.append(spread(-rates * soft))
        writes.append(spread(1.0 / (1.0 + jnp.exp(-pre_write))))
        q, k = piece_of(0, at) * inverse, piece_of(1, at) * inverse
        q_factor = unit_factor(q * q) * hs ** (-0.5)
        k_factor = unit_factor(k * k)
        queries.append(q * q_factor)
        keys.append(k * k_factor)
        gates.append(piece_of(2, at) * inverse)
        values.append(piece_of(3, at) * inverse)
        reads_q.append(load_rows(reads, pl.ds(p, seqs, stride=8)) * (q_factor * inverse))
        reads_k.append(load_rows(reads, pl.ds(props + p, seqs, stride=8)) * (k_factor * inverse))
    totals, fresh = updates(keys, values, log_decay, writes, reads_k)
    head_scale = by_head(lambda h: jnp.broadcast_to(head_gain[...].astype(F32), (seqs, hs)))
    for p in range(props):
        out = jnp.exp(totals[p]) * reads_q[p]
        for e in range(p + 1):
            out = out + jnp.exp(totals[p] - totals[e]) * head_sums(queries[p] * keys[e]) * fresh[e]
        out = out * lax.rsqrt(head_sums(out * out) * (1.0 / hs) + EPSILON)
        gate = gates[p]
        out = out * head_scale * (gate / (1.0 + jnp.exp(-gate)))
        store_rows(heads_f32, pl.ds(p, seqs, stride=props), out)

    per_tp = mine // tps
    for t in range(tps):
        heads_bf[t] = load_rows(heads_f32, pl.ds(t * per_tp, per_tp)).astype(BF16)
    head_copies = []
    for step in range(1, tps):
        copy = remote(
            heads_bf.at[tp_at(step)], gathered.at[kv, tp], head_send.at[step - 1], head_recv.at[step - 1],
            tp=tp_at(step),
        )
        copy.start()
        head_copies.append(copy)
    gathered[kv, tp] = heads_bf[tp]
    for copy in head_copies:
        copy.wait_recv()

    relays = {}
    twins = []

    def to_twin(who, n):
        copy = remote(gathered.at[who], gathered.at[who], twin_send.at[n], twin_recv.at[n], kv=twin)
        copy.start()
        twins.append(copy)

    reach = (half, zs - 1 - half)
    ahead = lax.rem(1 - 2 * core + zs, zs)
    for hop in range(0, half, RELAY):
        for side in range(2):
            if hop >= reach[side] or (hop == 0 and side == 1 and False):
                continue
            sign = 1 - 2 * side
            from_kv = lax.rem(z + (zs - hop) * sign * (1 - 2 * core) + 2 * zs * zs, zs) * 2 + core
            if hop > 0:
                relays[side, hop].wait_recv()
            for far in range(RELAY, 0, -1):
                if hop + far > reach[side]:
                    continue
                to = lax.rem(z + sign * (1 - 2 * core) * far + zs, zs) * 2 + core
                copy = remote(
                    gathered.at[from_kv], gathered.at[from_kv],
                    relay_send.at[side, hop + far - 1], relay_recv.at[side, hop + far - 1], kv=to,
                )
                copy.start()
                relays[side, hop + far] = copy
        if hop == 0:
            to_twin(kv, 0)
        for side in range(2):
            sign = 1 - 2 * side
            for far in range(1, RELAY + 1) if hop > 0 else ():
                at_hop = hop - RELAY + far
                if at_hop > reach[side]:
                    continue
                if at_hop % RELAY or at_hop + RELAY > half or at_hop >= reach[side]:
                    relays[side, at_hop].wait_recv()
                who = lax.rem(z - at_hop * sign * (1 - 2 * core) + 2 * zs, zs) * 2 + core
                to_twin(who, len(twins))
    for side in range(2):
        sign = 1 - 2 * side
        for at_hop in range(half - RELAY + 1, reach[side] + 1):
            relays[side, at_hop].wait_recv()
            who = lax.rem(z - at_hop * sign * (1 - 2 * core) + 2 * zs, zs) * 2 + core
            to_twin(who, len(twins))
    for copy in twins:
        copy.wait_recv()
    for copy in w_copies:
        copy.wait_recv()

    for c in range(zs):
        for t in range(tps):
            both = jnp.concatenate(
                [gathered[2 * c, t].astype(F32), gathered[2 * c + 1, t].astype(F32)], axis=0
            )
            flat[c * 2 * per_tp:(c + 1) * 2 * per_tp, t * width:(t + 1) * width] = both.astype(BF16)
    total = dot(flat[:, 0:width], w_out_all[0])
    for t in range(1, tps):
        total = total + dot(flat[:, t * width:(t + 1) * width], w_out_all[t])
    result[...] = total.reshape(result.shape).astype(BF16)
    mix_copies = []
    for step in range(1, tps):
        copy = remote(result, mixed.at[:, tp], mix_send.at[step - 1], mix_recv.at[step - 1], tp=tp_at(step))
        copy.start()
        mix_copies.append(copy)
    own = pltpu.make_async_copy(result, mixed.at[:, tp], store_sem.at[seqs])
    own.start()

    for copy in ring.values():
        copy.wait_send()
    for copy in w_copies + head_copies + list(relays.values()) + twins:
        copy.wait_send()
    for copy in stores:
        copy.wait()
    own.wait()
    for copy in mix_copies:
        copy.wait()


def per_device(
    sizes,
    hidden, norm_gain, w_query, w_key, w_value, w_gate, w_decay, w_write, decay_rate, head_gain, w_output,
    state, prev_keys, prev_values, prev_decay, prev_write, accepted,
):
    zs, tps = sizes
    tokens, feats = hidden.shape
    heads, width = w_decay.shape[1], w_query.shape[1]
    hs = width // heads
    seqs, props = prev_keys.shape[:2]
    rows = tokens // zs
    half = zs // 2
    part = 2 * width // PIECES
    per_tp = seqs * props // tps
    taken = (jnp.arange(props, dtype=jnp.int32)[None, :] < accepted[:, None])[..., None]
    old_scalars = jnp.concatenate(
        [jnp.where(taken, prev_decay, 0.0).reshape(seqs, -1), jnp.where(taken, prev_write, 0.0).reshape(seqs, -1)],
        axis=1,
    )
    lines = state.reshape(seqs, heads, hs, hs).transpose(0, 2, 1, 3).reshape(seqs * heads * hs, hs)
    any_ = pl.BlockSpec(memory_space=pl.ANY)
    vmem = pl.BlockSpec(memory_space=pltpu.VMEM)
    dma = pltpu.SemaphoreType.DMA
    scratch = [
        pltpu.VMEM((2, tokens, feats), BF16),
        pltpu.VMEM((norm_gain.shape[0] // feats, feats), F32),
        pltpu.VMEM((tokens, 2 * feats), BF16),
        pltpu.VMEM((2 * feats, 2 * width), BF16),
        pltpu.VMEM((feats, 2 * width), BF16),
        pltpu.VMEM((2, tokens, 2 * feats), BF16),
        pltpu.VMEM((8, 2 * feats), F32),
        pltpu.VMEM((2, rows, 2 * width), F32),
        pltpu.VMEM((half, 2, PIECES, rows, part), BF16),
        pltpu.VMEM((half, 2, PIECES, rows, part), BF16),
        pltpu.VMEM((max(WIDE_HOPS, 1), 2, PIECES // 2, rows, part), F32),
        pltpu.VMEM((max(WIDE_HOPS, 1), 2, PIECES // 2, rows, part), F32),
        pltpu.VMEM((half, 2, 8, rows), F32),
        pltpu.VMEM((half, 2, 8, rows), F32),
        pltpu.VMEM((2, 2 * heads, rows // 2, hs), F32),
        pltpu.VMEM((2, 2 * heads, rows // 2, hs), F32),
        pltpu.VMEM((2, 8, 128), F32),
        pltpu.VMEM((2, 128, 128), F32),
        pltpu.VMEM(lines.shape, F32),
        pltpu.VMEM((seqs * heads, hs, hs), BF16),
        pltpu.VMEM((seqs * heads, hs, hs), BF16),
        pltpu.VMEM(lines.shape, F32),
        pltpu.VMEM((heads, seqs * props, hs), F32),
        pltpu.VMEM((heads, seqs * props, hs), F32),
        pltpu.VMEM((heads, seqs * 8, hs), F32),
        pltpu.VMEM((heads, seqs * props, hs), F32),
        pltpu.VMEM((heads, seqs * props + seqs, hs), F32),
        pltpu.VMEM((heads, seqs * props, hs), F32),
        pltpu.VMEM((tps, per_tp, width), BF16),
        pltpu.VMEM((2 * zs, tps, per_tp, width), BF16),
        pltpu.VMEM((2 * zs * per_tp, tps * width), BF16),
        pltpu.VMEM((tps,) + w_output.shape, BF16),
        pltpu.VMEM((2 * zs, per_tp, w_output.shape[1]), BF16),
        dma((7,)), dma((2,)), dma((2,)),
        dma((half, 2, PIECES + 1)), dma((half, 2, PIECES + 1)),
        dma((PIECES + 1,)), dma((PIECES + 1,)),
        dma((tps - 1,)), dma((tps - 1,)),
        dma((tps - 1,)), dma((tps - 1,)),
        dma((2, half)), dma((2, half)),
        dma((zs,)), dma((zs,)),
        dma((tps - 1,)), dma((tps - 1,)),
        dma((seqs + 1,)),
    ]
    mixed, new_lines = pl.pallas_call(
        functools.partial(body, (zs, tps, seqs, props, heads, hs)),
        out_shape=(
            jax.ShapeDtypeStruct((2 * zs, tps, per_tp, w_output.shape[1]), BF16),
            jax.ShapeDtypeStruct(lines.shape, F32),
        ),
        in_specs=[any_, vmem, any_, any_, any_, any_, vmem, vmem, vmem, vmem, any_, any_, vmem, vmem, vmem],
        out_specs=(any_, any_),
        scratch_shapes=scratch,
        compiler_params=pltpu.CompilerParams(
            collective_id=0, has_side_effects=True, vmem_limit_bytes=40 * 1024 * 1024
        ),
    )(
        hidden, norm_gain.reshape(-1, feats), w_query, w_key, w_value, w_gate, w_decay.T, w_write.T,
        decay_rate.reshape(1, heads), head_gain.reshape(1, hs), w_output, lines, prev_keys, prev_values, old_scalars,
    )
    mixed = mixed.reshape(tokens, w_output.shape[1])
    new_state = new_lines.reshape(seqs, hs, heads, hs).transpose(0, 2, 1, 3).reshape(state.shape)
    return mixed, new_state


def solution(mesh):
    sizes = (mesh.shape["kv"] // 2, mesh.shape["tp"])
    in_specs = (
        P("grp", "kv"),
        P(),
        P("kv", "tp"),
        P("kv", "tp"),
        P("kv", "tp"),
        P("kv", "tp"),
        P(None, "tp"),
        P(None, "tp"),
        P("tp"),
        P(),
        P("tp", "kv"),
        P(GRP_KV, "tp", None),
        P(GRP_KV, None, "tp"),
        P(GRP_KV, None, "tp"),
        P(GRP_KV, None, "tp"),
        P(GRP_KV, None, "tp"),
        P(GRP_KV),
    )
    out_specs = (P("grp", "kv"), P(GRP_KV, "tp", None))
    return jax.shard_map(
        functools.partial(per_device, sizes), mesh=mesh, in_specs=in_specs, out_specs=out_specs, check_vma=False
    )
```

time: 252 us -> 104 us (0.41)
  waiting for transfers between devices: 129 us -> 0 us
  Pallas kernels: 0 us -> 85.6 us
  blocking collectives: 33.1 us -> 0 us
  starting transfers between devices: 29.5 us -> 0 us
  matrix products: 25.2 us -> 0 us
  between operations: 14.6 us -> 0.66 us
  other arithmetic: 7.45 us -> 1.46 us
  local copies, waits for them, and re-layouts: 11 us -> 14.3 us
    all_gather x2 -> x0, waiting for transfers between devices: 92.9 us -> none  [the longest x1 75.7 us: side_by_side(): lax.all_gather(both, axis, axis=dim, tiled=True)]
    pallas_call x0 -> x1, Pallas kernels: none -> 85.6 us  [per_device(): pl.pallas_call(functools.partial(body, (zs, tps, seqs, props, heads, hs))...]
    all_to_all x2 -> x0, waiting for transfers between devices: 35.8 us -> none  [the longest x1 25.2 us: from_everyone(): return lax.all_to_all(copies, axis, split_axis=0, concat_axis=0, tiled=True)]
    all_gather x1 -> x0, blocking collectives: 33.1 us -> none  [gather_in_order(): tiles = lax.all_gather(tiles, axes[k], axis=0, tiled=True)]
    all_to_all x2 -> x0, starting transfers between devices: 29.4 us -> none  [the longest x1 24.8 us: per_device(): lax.all_to_all(hidden, KV, split_axis=0, concat_axis=1, tiled=True)]
    dot_general x14 -> x0, matrix products: 25.2 us -> none  [the longest x4 12 us: per_device(): jnp.dot(scaled, piece, preferred_element_type=jnp.float32)]
    unnamed x24 -> x30, local copies, waits for them, and re-layouts: 0.06 us -> 14.1 us
    reshape x8 -> x2, local copies, waits for them, and re-layouts: 4.82 us -> 0.14 us  [the longest x1 0.07 us: per_device(): jnp.where(taken, prev_decay, 0.0).reshape(seqs, -1)]
  transfers between devices with their start and end apart: 4 -> 0, of which waited for: 4 -> 0; matrix products, arithmetic and copies ran while one was open for 6% -> 0% of each run, Pallas kernels for 0% -> 0%
where the time goes in v1:
time: 104 us; the launch traced here: 102 us
  Pallas kernels  85.6 us (82%)
  local copies, waits for them, and re-layouts  14.3 us (14%)
  other arithmetic  1.46 us (1%)
    pallas_call x1, Pallas kernels, per_device(): pl.pallas_call(functools.partial(body, (zs, tps, seqs, props, heads, hs))...  85.6 us
    unnamed x30, local copies, waits for them, and re-layouts  14.1 us

profile of v1, /device:TPU:40, one launch (start us, length us, event | category | flops | bytes accessed | tf_op | source)
XLA Modules:
  0.0 101.9 jit_solution(7775682125567921754)
XLA Ops:
  0.6 0.7 iota_compare_fusion
  1.3 0.7 broadcast_select_fusion.1
  2.0 0.1 copy.20
  2.1 0.1 copy.21
  2.1 0.1 pad_maximum_fusion.old_scalars
  2.2 0.0 copy-start
  2.2 1.6 %copy-done = f32[8,4,16384]{2,1,0:T(4,128)S(1)} copy-done((f32[8,4,16384]{2,1,0:T(4,128)S(1)}, f32[8,4,16384]{2,1,0:T(4,128)}, u32[]{:S(2)}) %copy-start) | copy-done | bytes 2097176
  3.8 0.0 copy-start.1
  3.8 0.9 copy-done.1
  4.8 0.0 copy-start.2
  4.8 0.9 copy-done.2
  5.7 0.0 copy-start.3
  5.7 0.9 copy-done.3
  6.6 0.0 copy-start.4
  6.6 0.9 copy-done.4
  7.5 0.0 copy-start.5
  7.5 0.9 copy-done.5
  8.4 0.0 copy-start.6
  8.4 0.9 copy-done.6
  9.3 0.0 copy-start.7
  9.3 0.8 copy-done.7
  10.1 0.0 copy-start.8
  10.1 0.8 copy-done.8
  10.8 0.0 copy-start.9
  10.8 0.8 copy-done.9
  11.6 0.0 copy-start.10
  11.6 0.8 copy-done.10
  12.3 0.0 copy-start.11
  12.3 0.7 copy-done.11
  13.0 0.0 copy-start.12
  13.0 0.7 copy-done.12
  13.7 0.0 copy-start.13
  13.7 0.7 copy-done.13
  14.3 85.6 %shard_map.176 = (bf16[32,4,8,128]{3,2,1,0:T(8,128)(2,1)S(1)}, f32[4096,128]{1,0:T(8,128)S(1)}) custom-call(bf16[1024,128]{1,0:T(8,128)(2,1)S(1)} %copy-done.1, bf16[32,128]{1,0:T(8,128)(2,1)S(1)} %bitcast.23, bf16[128,512]{1,0:T(8,128)(2,1)S(1)} %copy-done.2, bf16[128,512]{1,0:T(8,128)(2,1)S(1)} %copy-done.3, bf16[128,512]{1,0:T(8,128)(2,1)S(1)} %copy-done.4, ...), custom_call_target="tpu_custom_call" | custom-call | tf_op jit(solution)/shard_map/pallas_call | solution.py:554
  99.9 0.7 copy.25
  100.6 1.3 %copy.26 = f32[8,4,16384]{2,1,0:T(4,128)} copy(f32[8,4,16384]{2,1,0:T(4,128)S(1)} %bitcast.19) | data formatting | bytes 4194304
Async XLA Ops:
  2.2 1.6 %copy-start = (f32[8,4,16384]{2,1,0:T(4,128)S(1)}, f32[8,4,16384]{2,1,0:T(4,128)}, u32[]{:S(2)}) copy-start(f32[8,4,16384]{2,1,0:T(4,128)} %param.28) | copy-start | bytes 6291460
  3.8 0.9 copy-start.1
  4.8 0.9 copy-start.2
  5.7 0.9 copy-start.3
  6.6 0.9 copy-start.4
  7.5 0.9 copy-start.5
  8.4 0.9 copy-start.6
  9.3 0.8 copy-start.7
  10.1 0.8 copy-start.8
  10.8 0.8 copy-start.9
  11.6 0.8 copy-start.10
  12.3 0.7 copy-start.11
  13.0 0.7 copy-start.12
  13.7 0.7 copy-start.13
